TPU v7x, 512 devices: a whole 4x4x16 slice. The times are simulated.
512 devices in a mesh: ep: 32 (over z, core), tp: 16 (over y, x).
Axes of the slice: x: 4, y: 4, z: 16, core: 2. Of those that a mesh axis runs over, the one named last changes fastest.
Arguments:
- mixer_rows: bfloat16 [8192, 2048], P('ep'), may hold values from -8 to 8
- mixer_gain: float32 [2048], replicated, may hold values from 0.1 to 1.9
- w_query: bfloat16 [2048, 1024], P(None, 'tp'), may hold values from -0.125 to 0.125
- w_key: bfloat16 [2048, 1024], P(None, 'tp'), may hold values from -0.125 to 0.125
- w_value: bfloat16 [2048, 1024], P(None, 'tp'), may hold values from -0.125 to 0.125
- key_shift: float32 [16, 8192], P('tp'), may hold values from -14 to 0
- w_out: bfloat16 [1024, 2048], P(None, 'tp'), may hold values from -0.75 to 0.75
- expert_rows: bfloat16 [4096, 2048], P('ep'), may hold values from -6 to 6
- expert_gain: float32 [2048], replicated, may hold values from 0.1 to 1.9
- routes: int32 [4096, 4], P('ep'), may hold values from 0 to 31, all different within a row; in each aligned block of 128 rows (0 to 127, 128 to 255, ...) at most 32 rows name the same one
- route_weight: float32 [4096, 4], P('ep'), may hold values from 0.05 to 0.6
- w_gate: bfloat16 [32, 2048, 2048], P('ep', None, 'tp'), may hold values from -0.25 to 0.25
- w_up: bfloat16 [32, 2048, 2048], P('ep', None, 'tp'), may hold values from -0.25 to 0.25
- w_down: bfloat16 [32, 2048, 2048], P('ep', None, 'tp'), may hold values from -0.0625 to 0.0625
Outputs:
- mixer_out: bfloat16 [8192, 2048], P('ep', 'tp')
- expert_out: bfloat16 [4096, 2048], P('ep', 'tp')
Inputs may be any that keep to these rules, and one draw needn't show every extreme that they name: `routes`: each row names 4 different experts. In each aligned block of 128 rows no expert is named by more than 32 rows, and in every draw some block names some expert exactly 32 times.
All inputs are finite; a program needn't handle non-finite values.
Results may differ from a plain program's by a relative error of at most 0.0073.
Values may be sent and summed in bfloat16 or wider, within the bound.
A program may use at most 64 MiB of HBM per device.

v0:
```python
import jax
import jax.numpy as jnp
from jax import lax
from jax.sharding import Mesh
from jax.sharding import PartitionSpec as P

EP = ("ep_0", "ep_1")
norm_eps = 1e-06
glu_limit = 7.0
glu_alpha = 1.702


def in_order(blocks, dim):
    shape = list(blocks.shape[1:])
    shape[dim] *= blocks.shape[0]
    return jnp.moveaxis(blocks, 0, dim).reshape(shape)


def all_blocks(shard, axes, turns):
    blocks = shard[None]
    for k in turns:
        blocks = lax.all_gather(blocks, axes[k], axis=0, tiled=True)
    carried = [lax.axis_size(axes[k]) for k in reversed(turns)]
    blocks = blocks.reshape(*carried, *shard.shape)
    turned = sorted(range(len(turns)), key=lambda place: turns[len(turns) - 1 - place])
    return blocks.transpose(*turned, *range(len(turns), blocks.ndim)).reshape(-1, *shard.shape)


def whole_of(shard, axes, turns, dim):
    return in_order(all_blocks(shard, axes, turns), dim)


def copy_for_each(shard, axis):
    devices = lax.axis_size(axis)
    return lax.all_to_all(
        jnp.broadcast_to(shard[None], (devices, *shard.shape)), axis, 0, 0, tiled=True
    )


def gather_directly(shard, axis, dim):
    blocks = copy_for_each(shard, axis)
    return in_order(blocks, dim)


def rms_scale(source, scaling):
    floats = source.astype(jnp.float32)
    inverse = lax.rsqrt(jnp.mean(floats * floats, axis=-1, keepdims=True) + norm_eps)
    return (floats * inverse * scaling).astype(jnp.bfloat16)


def stick_block(queries, packed, shifting, carried, allowed):
    length, head_count, head_width = queries.shape
    key_part = packed[:, : head_count * head_width].reshape(length, head_count, head_width)
    value_part = packed[:, head_count * head_width :].reshape(length, head_count, head_width)
    scores = jnp.einsum("thd,shd->hts", queries, key_part, preferred_element_type=jnp.float32)
    scores = scores * head_width ** (-0.5) + shifting[:, None, :]
    log_stay = jnp.where(allowed, jax.nn.log_sigmoid(-scores), 0.0)
    between = lax.cumsum(log_stay, axis=2, reverse=True) - log_stay
    weights = jnp.where(
        allowed, jnp.exp(jax.nn.log_sigmoid(scores) + between + carried[:, :, None]), 0.0
    )
    contrib = jnp.einsum(
        "hts,shd->thd", weights.astype(jnp.bfloat16), value_part, preferred_element_type=jnp.float32
    )
    return (contrib, carried + jnp.sum(log_stay, axis=2))


def per_device(
    mixer_rows,
    mixer_gain,
    w_query,
    w_key,
    w_value,
    key_shift,
    w_out,
    expert_rows,
    expert_gain,
    routes,
    route_weight,
    w_gate,
    w_up,
    w_down,
):
    length = mixer_rows.shape[0]
    head_count = key_shift.shape[0]
    head_width = w_query.shape[1] // head_count
    normed = rms_scale(mixer_rows, mixer_gain)
    queries = jnp.dot(normed, w_query, preferred_element_type=jnp.float32).astype(jnp.bfloat16)
    key_rows = jnp.dot(normed, w_key, preferred_element_type=jnp.float32).astype(jnp.bfloat16)
    value_rows = jnp.dot(normed, w_value, preferred_element_type=jnp.float32).astype(jnp.bfloat16)
    queries = queries.reshape(length, head_count, head_width)
    packed = jnp.concatenate([key_rows, value_rows], axis=1)
    device = lax.axis_index(EP)
    positions = jnp.arange(length, dtype=jnp.int32)
    strict = (positions[None, :] < positions[:, None])[None]
    own_shift = lax.dynamic_slice_in_dim(key_shift, device * length, length, 1)
    summed, carried = stick_block(
        queries, packed, own_shift, jnp.zeros((head_count, length), jnp.float32), strict
    )
    gathered = whole_of(packed, EP, (0, 1), 0)

    def visiting(offset, status):
        running, carry_now = status
        anchor = device - offset
        block_rows = lax.dynamic_slice_in_dim(gathered, anchor * length, length, 0)
        shifting = lax.dynamic_slice_in_dim(key_shift, anchor * length, length, 1)
        contrib, carry_now = stick_block(queries, block_rows, shifting, carry_now, True)
        return (running + contrib, carry_now)

    summed, carried = lax.fori_loop(1, device + 1, visiting, (summed, carried))
    head_out = summed.reshape(length, head_count * head_width).astype(jnp.bfloat16)
    weight_rows = w_out
    mixer_out = jnp.dot(
        gather_directly(head_out, "tp", 1), weight_rows, preferred_element_type=jnp.float32
    ).astype(jnp.bfloat16)
    tokens_here, top_count = routes.shape
    expert_count = lax.axis_size(EP)
    capacity = 2 * tokens_here * top_count // expert_count
    rows_after_norm = rms_scale(expert_rows, expert_gain)
    chosen = routes.reshape(-1)
    hit_table = (chosen[:, None] == jnp.arange(expert_count, dtype=jnp.int32)[None, :]).astype(
        jnp.int32
    )
    places = jnp.sum((jnp.cumsum(hit_table, axis=0) - 1) * hit_table, axis=1)
    targets = chosen * capacity + places
    assign_ids = jnp.arange(tokens_here * top_count, dtype=jnp.int32) // top_count
    owners = (
        jnp.full((expert_count * capacity,), tokens_here, jnp.int32).at[targets].set(assign_ids)
    )
    padded = jnp.concatenate(
        [rows_after_norm, jnp.zeros((1, rows_after_norm.shape[1]), jnp.bfloat16)], axis=0
    )
    outgoing = padded[owners].reshape(expert_count, capacity, rows_after_norm.shape[1])
    gate_cols = w_gate[0]
    upper_cols = w_up[0]
    down_rows = w_down[0]
    portion_size = capacity // lax.axis_size("tp")
    own_slots = lax.dynamic_slice_in_dim(
        outgoing, lax.axis_index("tp") * portion_size, portion_size, 1
    )
    arrived = lax.all_to_all(own_slots, EP, split_axis=0, concat_axis=0, tiled=True)
    expert_arrived = lax.all_gather(arrived, "tp", axis=1, tiled=True)
    expert_senders, slots_here, feature_count = expert_arrived.shape
    flat_rows = expert_arrived.reshape(expert_senders * slots_here, feature_count)
    gating = jnp.minimum(
        jnp.dot(flat_rows, gate_cols, preferred_element_type=jnp.float32), glu_limit
    )
    linear = jnp.clip(
        jnp.dot(flat_rows, upper_cols, preferred_element_type=jnp.float32), -glu_limit, glu_limit
    )
    hidden = gating * jax.nn.sigmoid(glu_alpha * gating) * (linear + 1.0)
    hidden = hidden.astype(jnp.bfloat16).reshape(expert_senders, slots_here, gate_cols.shape[1])
    senders = hidden.shape[0]
    slot_total = hidden.shape[1]
    portion_units = lax.all_gather(hidden, "tp", axis=2, tiled=True)
    weight_rows = down_rows
    flat_units = portion_units.reshape(senders * slot_total, portion_units.shape[2])
    results = jnp.dot(flat_units, weight_rows, preferred_element_type=jnp.float32)
    leaving = results.astype(jnp.bfloat16).reshape(senders, slot_total, down_rows.shape[1])
    returned = lax.all_to_all(leaving, EP, split_axis=0, concat_axis=0, tiled=True)
    picked = returned.reshape(expert_count * capacity, down_rows.shape[1])[targets].astype(
        jnp.float32
    )
    picked = picked * route_weight.reshape(-1)[:, None]
    expert_out = jnp.sum(picked.reshape(tokens_here, top_count, down_rows.shape[1]), axis=1).astype(
        jnp.bfloat16
    )
    return (mixer_out, expert_out)


def solution(mesh):
    torus = Mesh(mesh.devices.reshape(16, 2, mesh.shape["tp"]), ("ep_0", "ep_1", "tp"))
    return jax.shard_map(
        per_device,
        mesh=torus,
        in_specs=(
            P(EP, None),
            P(),
            P(None, "tp"),
            P(None, "tp"),
            P(None, "tp"),
            P("tp", None),
            P(None, "tp"),
            P(EP, None),
            P(),
            P(EP, None),
            P(EP, None),
            P(EP, None, "tp"),
            P(EP, None, "tp"),
            P(EP, None, "tp"),
        ),
        out_specs=(P(EP, "tp"), P(EP, "tp")),
        check_vma=False,
    )
```

profile of v0, /device:TPU:1, one launch (start us, length us, event | category | flops | bytes accessed | tf_op | source)
XLA Modules:
  0.0 366.4 jit_solution(1222065985565656454)
XLA Ops:
  7.3 1.6 fusion.17
  8.9 1.8 convolution_convert_fusion.2
  10.8 0.5 convolution_convert_fusion.4
  11.3 0.6 pad_maximum_fusion
  12.0 0.1 copy.63
  12.3 0.2 fusion.24
  12.5 1.2 reduce-window.26
  13.6 0.2 fusion.26
  13.9 0.2 slice_reduce_fusion
  14.1 0.1 eq.25
  14.2 0.1 copy.62
  14.3 0.1 mul.115
  14.6 2.4 scatter_custom_fusion
  17.1 6.0 %gather_fusion = bf16[1024,2048]{1,0:T(8,128)(2,1)} fusion(bf16[129,2048]{1,0:T(8,128)(2,1)S(1)} %concatenate.7, s32[1024]{0:T(1024)S(1)} %fusion.44), kind=kCustom, calls=%fused_computation | custom fusion | bytes 8392704 | tf_op jit(solution)/shard_map/gather | solution.py:133
  23.1 1.5 constant_dynamic-slice_fusion.1
  24.6 40.3 %all_to_all.15 = bf16[32,2,2048]{2,1,0:T(2,128)(2,1)S(1)} all-to-all(bf16[32,2,2048]{2,1,0:T(2,128)(2,1)S(1)} %constant_dynamic-slice_fusion.1), channel_id=1, replica_groups=mesh['ep_0'=16,'ep_1'=2,'tp'=16] {'ep_0','ep_1'}, dimensions={0} | all-to-all | bytes 524288 | tf_op jit(solution)/shard_map/all_to_all | solution.py:141
  64.9 0.8 copy.66
  65.8 19.3 %all-gather.12.cloned.1.call-done = bf16[4096,128]{0,1:T(8,128)(2,1)} async-done(((bf16[256,128]{0,1:T(8,128)(2,1)}), bf16[4096,128]{0,1:T(8,128)(2,1)}) %all-gather.12.cloned.1.call-update) | async-done | bytes 1048592 | tf_op jit(solution)/shard_map/all_gather | solution.py:22
  85.1 2.5 copy.70
  87.6 0.2 all-gather.10.cloned.1.call-start
  87.8 72.1 %all-gather.8.cloned.1.call-done = bf16[32,32,2048]{2,0,1:T(8,128)(2,1)} async-done(((bf16[32,2,2048]{2,0,1:T(8,128)(2,1)}), bf16[32,32,2048]{2,0,1:T(8,128)(2,1)}) %all-gather.8.cloned.1.call-update) | async-done | bytes 4194320 | tf_op jit(solution)/shard_map/all_gather | solution.py:142
  159.9 4.5 %copy.67 = bf16[32,32,2048]{2,1,0:T(8,128)(2,1)S(1)} copy(bf16[32,32,2048]{2,0,1:T(8,128)(2,1)} %all-gather.8.cloned.1.call-done) | data formatting | bytes 8388608 | tf_op jit(solution)/shard_map/all_gather | solution.py:142
  164.4 1.3 convolution_minimum_fusion
  165.7 2.0 fusion.22
  167.7 0.7 constant_dynamic-slice_fusion.2
  168.4 0.5 convolution_convert_fusion.3
  168.9 0.4 fusion.50
  169.3 2.3 fusion.39
  171.6 0.3 fusion.34
  171.9 0.1 convolution_bitcast_fusion.1
  172.1 12.4 %all-gather.6.cloned.1.call-done = bf16[32,256,128]{1,0,2:T(8,128)(2,1)} async-done(((bf16[16,256,128]{1,0,2:T(8,128)(2,1)}), bf16[32,256,128]{1,0,2:T(8,128)(2,1)}) %all-gather.6.cloned.1.call-update) | async-done | bytes 2097168 | tf_op jit(solution)/shard_map/all_gather | solution.py:22
  184.5 3.5 copy.61
  187.9 4.1 %while.12 = (s32[]{:T(128)}, f32[256,1,64]{0,2,1:T(8,128)S(1)}, f32[1,256]{1,0:T(1,128)S(1)}, s32[]{:T(128)}, s32[]{:T(128)}, /*index=5*/bf16[8192,128]{1,0:T(8,...) while((s32[]{:T(128)}, f32[256,1,64]{0,2,1:T(8,128)S(1)}, ...), condition=%wide.region_8.9_spmd, body=%wide.region_4.8_spmd.sunk | while | flops 27083784 | bytes 2680031 | solution.py:110
  188.0 0.7 constant_dynamic-slice_fusion.4
  188.7 0.3 fusion.77
  189.0 2.3 fusion.78
  191.4 0.4 fusion.79
  191.7 0.3 fusion.80
  192.1 0.8 broadcast_in_dim.17
  192.9 5.5 %all-to-all-start = ((bf16[16,256,64]{1,2,0:T(8,128)(2,1)}), bf16[16,256,64]{1,2,0:T(8,128)(2,1)S(1)}, u32[]{:S(2)}, u32[]{:S(2)}) async-start(bf16[16,256,64]{1,2,0:T(8,128)(2,1)} %broadcast_in_dim.17), calls=%async_computation | async-start | bytes 1048576 | tf_op jit(solution)/shard_map/all_to_all | solution.py:35
  198.4 59.6 %all-gather.10.cloned.1.call-done = bf16[32,32,2048]{2,1,0:T(8,128)(2,1)} async-done(((bf16[32,32,128]{2,1,0:T(8,128)(2,1)}), bf16[32,32,2048]{2,1,0:T(8,128)(2,1)}) %all-gather.10.cloned.1.call-update) | async-done | bytes 4194320 | tf_op jit(solution)/shard_map/all_gather | solution.py:155
  258.0 4.3 %convolution_convert_fusion = bf16[1024,128]{1,0:T(8,128)(2,1)} fusion(bf16[1024,2048]{1,0:T(8,128)(2,1)} %bitcast.152, bf16[1,2048,128]{2,1,0:T(8,128)(2,1)} %param.29), kind=kOutput, calls=%fused_computation.40 | convolution fusion | flops 537001984 | bytes 4980736 | tf_op jit(solution)/shard_map/dot_general | solution.py:158
  262.3 73.1 %all-to-all-start.2 = ((bf16[32,32,128]{2,1,0:T(8,128)(2,1)}), bf16[32,32,128]{2,1,0:T(8,128)(2,1)S(1)}, u32[]{:S(2)}, u32[]{:S(2)}) async-start(bf16[32,32,128]{2,1,0:T(8,128)(2,1)} %bitcast.38), calls=%async_computation.2 | async-start | bytes 524288 | tf_op jit(solution)/shard_map/all_to_all | solution.py:160
  335.4 0.1 copy.68
  335.5 1.0 convolution_convert_fusion.1
  336.5 21.1 %all-to-all-done.2 = bf16[32,32,128]{2,1,0:T(8,128)(2,1)S(1)} async-done(((bf16[32,32,128]{2,1,0:T(8,128)(2,1)}), bf16[32,32,128]{2,1,0:T(8,128)(2,1)S(1)}, u32[]{:S(2)}, u32[]{:S(2)}) %all-to-all-start.2) | async-done | bytes 262176 | tf_op jit(solution)/shard_map/all_to_all | solution.py:160
  357.6 1.3 gather_fusion.1
  359.0 0.9 fusion.37
  (54 shorter events, 0.7 us)
Async XLA Ops:
  7.2 157.2 %copy-start = (bf16[1,2048,128]{2,1,0:T(8,128)(2,1)S(1)}, bf16[1,2048,128]{2,1,0:T(8,128)(2,1)}, u32[]{:S(2)}) copy-start(bf16[1,2048,128]{2,1,0:T(8,128)(2,1)} %param.27) | copy-start | bytes 1572868
  7.2 3.6 copy-start.2
  7.2 3.6 copy-start.10
  7.2 3.6 copy-start.8
  7.2 77.9 %all-gather.12.cloned.1.call-start = ((), (), s32[]{:S(2)}) async-start(), calls=%async_computation.6 | async-start | bytes 1114112 | tf_op jit(solution)/shard_map/all_gather | solution.py:22
  8.9 3.1 copy-start.5
  8.9 3.4 copy-start.1
  10.8 2.9 copy-start.4
  12.0 147.9 %all-gather.8.cloned.1.call-start = ((), (), s32[]{:S(2)}) async-start(), calls=%async_computation.4 | async-start | bytes 4456448 | tf_op jit(solution)/shard_map/all_gather | solution.py:142
  65.8 118.7 %all-gather.6.cloned.1.call-start = ((), (), s32[]{:S(2)}) async-start(), calls=%async_computation.3 | async-start | bytes 3145728 | tf_op jit(solution)/shard_map/all_gather | solution.py:22
  87.6 170.4 %all-gather.10.cloned.1.call-start = ((), (), s32[]{:S(2)}) async-start(), calls=%async_computation.5 | async-start | bytes 4456448 | tf_op jit(solution)/shard_map/all_gather | solution.py:155
  164.4 1.3 copy-start.7
  165.7 2.7 copy-start.9
  192.9 69.4 %all-to-all-start = ((bf16[16,256,64]{1,2,0:T(8,128)(2,1)}), bf16[16,256,64]{1,2,0:T(8,128)(2,1)S(1)}, u32[]{:S(2)}, u32[]{:S(2)}) async-start(bf16[16,256,64]{1,2,0:T(8,128)(2,1)} %broadcast_in_dim.17), calls=%async_computation | async-start | bytes 1048576 | tf_op jit(solution)/shard_map/all_to_all | solution.py:35
  258.0 77.4 %copy-start.6 = (f32[128,4]{0,1:T(4,128)S(1)}, f32[128,4]{0,1:T(4,128)}, u32[]{:S(2)}) copy-start(f32[128,4]{0,1:T(4,128)} %param.26) | copy-start | bytes 6148
  258.0 77.5 %copy-start.3 = (bf16[1024,128]{1,0:T(8,128)(2,1)S(1)}, bf16[1024,128]{1,0:T(8,128)(2,1)}, u32[]{:S(2)}) copy-start(bf16[1024,128]{1,0:T(8,128)(2,1)} %param.22) | copy-start | bytes 786436
  262.3 95.3 %all-to-all-start.2 = ((bf16[32,32,128]{2,1,0:T(8,128)(2,1)}), bf16[32,32,128]{2,1,0:T(8,128)(2,1)S(1)}, u32[]{:S(2)}, u32[]{:S(2)}) async-start(bf16[32,32,128]{2,1,0:T(8,128)(2,1)} %bitcast.38), calls=%async_computation.2 | async-start | bytes 524288 | tf_op jit(solution)/shard_map/all_to_all | solution.py:160
Sparse Core Ops, SparseCore 0:
  12.1 72.9 all-gather.11
  88.1 71.7 all-gather.7
  162.0 22.4 all-gather.5
  187.3 70.6 all-gather.9
where the time goes:
time: 367 us; the launch traced here: 366 us
  waiting for transfers between devices  185 us (50%)
  starting transfers between devices  79 us (22%)
  blocking collectives  40.3 us (11%)
  local copies, waits for them, and re-layouts  25.8 us (7%)
  between operations  14.1 us (4%)
  matrix products  12.4 us (3%)
  other arithmetic  10.2 us (3%)
    all_to_all x1, starting transfers between devices, per_device(): lax.all_to_all(leaving, EP, split_axis=0, concat_axis=0, tiled=True)  73.1 us
    all_gather x1, waiting for transfers between devices, per_device(): expert_arrived = lax.all_gather(arrived, 'tp', axis=1, tiled=True)  72.1 us
    all_gather x1, waiting for transfers between devices, per_device(): portion_units = lax.all_gather(hidden, 'tp', axis=2, tiled=True)  59.6 us
    all_to_all x1, blocking collectives, per_device(): lax.all_to_all(own_slots, EP, split_axis=0, concat_axis=0, tiled=True)  40.3 us
    all_gather x2, waiting for transfers between devices, all_blocks(): blocks = lax.all_gather(blocks, axes[k], axis=0, tiled=True)  31.7 us
    all_to_all x1, waiting for transfers between devices, per_device(): lax.all_to_all(leaving, EP, split_axis=0, concat_axis=0, tiled=True)  21.1 us
  transfers between devices with their start and end apart: 6, of which 5 were waited for; matrix products, arithmetic and copies ran while one was open for 11% of the time, Pallas kernels for 0%

commit v1 on v0

--- a/solution.py
+++ b/solution.py
@@ -8,6 +8,14 @@
 norm_eps = 1e-06
 glu_limit = 7.0
 glu_alpha = 1.702
+
+
+def gather_from_all(array, axis, dim):
+    size = lax.axis_size(axis)
+    repeats = [size if d == dim else 1 for d in range(array.ndim)]
+    return lax.all_to_all(
+        jnp.tile(array, repeats), axis, split_axis=dim, concat_axis=dim, tiled=True
+    )
 
 
 def in_order(blocks, dim):
@@ -139,7 +147,7 @@
         outgoing, lax.axis_index("tp") * portion_size, portion_size, 1
     )
     arrived = lax.all_to_all(own_slots, EP, split_axis=0, concat_axis=0, tiled=True)
-    expert_arrived = lax.all_gather(arrived, "tp", axis=1, tiled=True)
+    expert_arrived = gather_from_all(arrived, "tp", 1)
     expert_senders, slots_here, feature_count = expert_arrived.shape
     flat_rows = expert_arrived.reshape(expert_senders * slots_here, feature_count)
     gating = jnp.minimum(

time: 367 us -> 344 us (0.937)
  blocking collectives: 40.3 us -> 0 us
  starting transfers between devices: 79 us -> 103 us
  waiting for transfers between devices: 185 us -> 174 us
    all_gather x1 -> x0, waiting for transfers between devices: 72.1 us -> none  [per_device(): expert_arrived = lax.all_gather(arrived, 'tp', axis=1, tiled=True)]
    all_to_all x1 -> x0, blocking collectives: 40.3 us -> none  [per_device(): lax.all_to_all(own_slots, EP, split_axis=0, concat_axis=0, tiled=True)]
    all_gather x2, waiting for transfers between devices: 31.7 us -> 69.4 us  [all_blocks(): blocks = lax.all_gather(blocks, axes[k], axis=0, tiled=True)]
    all_to_all x0 -> x2, starting transfers between devices: none -> 23.7 us  [the longest x1 16.7 us: per_device(): lax.all_to_all(own_slots, EP, split_axis=0, concat_axis=0, tiled=True)]
    all_to_all x0 -> x2, waiting for transfers between devices: none -> 23.6 us  [the longest x1 22 us: per_device(): lax.all_to_all(own_slots, EP, split_axis=0, concat_axis=0, tiled=True)]
    all_to_all x0 -> x1, local copies, waits for them, and re-layouts: none -> 4.49 us  [gather_from_all(): lax.all_to_all(jnp.tile(array, repeats), axis, split_axis=dim, concat_axi...]
    all_gather x1 -> x0, local copies, waits for them, and re-layouts: 4.49 us -> none  [per_device(): expert_arrived = lax.all_gather(arrived, 'tp', axis=1, tiled=True)]
  transfers between devices with their start and end apart: 6 -> 7, of which waited for: 5 -> 6; matrix products, arithmetic and copies ran while one was open for 11% -> 9% of each run, Pallas kernels for 0% -> 0%
where the time goes in v1:
time: 344 us; the launch traced here: 343 us
  waiting for transfers between devices  174 us (51%)
  starting transfers between devices  103 us (30%)
  local copies, waits for them, and re-layouts  29.4 us (9%)
  between operations  14 us (4%)
  other arithmetic  11.6 us (3%)
  matrix products  11.1 us (3%)
    all_to_all x1, starting transfers between devices, per_device(): lax.all_to_all(leaving, EP, split_axis=0, concat_axis=0, tiled=True)  73 us
    all_gather x2, waiting for transfers between devices, all_blocks(): blocks = lax.all_gather(blocks, axes[k], axis=0, tiled=True)  69.4 us
    all_gather x1, waiting for transfers between devices, per_device(): portion_units = lax.all_gather(hidden, 'tp', axis=2, tiled=True)  59.6 us
    all_to_all x1, waiting for transfers between devices, per_device(): lax.all_to_all(own_slots, EP, split_axis=0, concat_axis=0, tiled=True)  22 us
    all_to_all x1, waiting for transfers between devices, per_device(): lax.all_to_all(leaving, EP, split_axis=0, concat_axis=0, tiled=True)  21.1 us
    all_to_all x1, starting transfers between devices, per_device(): lax.all_to_all(own_slots, EP, split_axis=0, concat_axis=0, tiled=True)  16.7 us
    all_to_all x1, starting transfers between devices, gather_from_all(): lax.all_to_all(jnp.tile(array, repeats), axis, split_axis=dim, concat_axi...  6.94 us
  transfers between devices with their start and end apart: 7, of which 6 were waited for; matrix products, arithmetic and copies ran while one was open for 9% of the time, Pallas kernels for 0%

profile of v1, /device:TPU:1, one launch (start us, length us, event | category | flops | bytes accessed | tf_op | source)
XLA Modules:
  0.0 342.6 jit_solution(11334325279424873342)
XLA Ops:
  7.2 0.8 copy.51
  8.2 0.7 broadcast_multiply_fusion
  8.9 1.2 reduce-window.26
  10.1 0.2 slice_reduce_fusion
  10.7 2.4 scatter_custom_fusion
  13.2 1.2 fusion.24
  14.4 1.2 fusion.26
  15.7 6.0 %gather_fusion = bf16[1024,2048]{1,0:T(8,128)(2,1)} fusion(bf16[129,2048]{1,0:T(8,128)(2,1)S(1)} %concatenate.7, s32[1024]{0:T(1024)S(1)} %fusion.44), kind=kCustom, calls=%fused_computation | custom fusion | bytes 8392704 | tf_op jit(solution)/shard_map/gather | solution.py:141
  21.8 2.2 constant_dynamic-slice_fusion.1
  23.9 16.7 %all-to-all-start.1 = ((bf16[32,2,2048]{2,1,0:T(2,128)(2,1)}), bf16[32,2,2048]{2,1,0:T(2,128)(2,1)S(1)}, u32[]{:S(2)}, u32[]{:S(2)}) async-start(bf16[32,2,2048]{2,1,0:T(2,128)(2,1)} %constant_dynamic-slice_fusion.1), calls=%async_computation.1 | async-start | bytes 524288 | tf_op jit(solution)/shard_map/all_to_all | solution.py:149
  40.7 0.3 fusion.17
  41.0 22.0 %all-to-all-done.1 = bf16[32,2,2048]{2,1,0:T(2,128)(2,1)S(1)} async-done(((bf16[32,2,2048]{2,1,0:T(2,128)(2,1)}), bf16[32,2,2048]{2,1,0:T(2,128)(2,1)S(1)}, u32[]{:S(2)}, u32[]{:S(2)}) %all-to-all-start.1) | async-done | bytes 262176 | tf_op jit(solution)/shard_map/all_to_all | solution.py:149
  63.0 2.5 tile.4
  65.5 6.9 %all-to-all-start.2 = ((bf16[32,32,2048]{2,0,1:T(8,128)(2,1)}), bf16[32,32,2048]{2,0,1:T(8,128)(2,1)}, u32[]{:S(2)}, u32[]{:S(2)}) async-start(bf16[32,32,2048]{2,0,1:T(8,128)(2,1)} %bitcast.132), calls=%async_computation.2 | async-start | bytes 8388608 | tf_op jit(solution)/shard_map/all_to_all | solution.py:16
  72.6 0.5 convolution_convert_fusion.2
  73.1 0.3 copy-done.6
  73.4 0.5 convolution_convert_fusion.4
  73.9 0.6 pad_maximum_fusion
  74.7 55.9 %all-gather.9.cloned.1.call-done = bf16[4096,128]{0,1:T(8,128)(2,1)} async-done(((bf16[256,128]{0,1:T(8,128)(2,1)}), bf16[4096,128]{0,1:T(8,128)(2,1)}) %all-gather.9.cloned.1.call-update) | async-done | bytes 1048592 | tf_op jit(solution)/shard_map/all_gather | solution.py:30
  130.6 2.5 copy.58
  133.1 0.2 all-gather.7.cloned.1.call-start
  133.3 1.7 all-to-all-done.2
  135.0 4.5 %copy.55 = bf16[32,32,2048]{2,1,0:T(8,128)(2,1)S(1)} copy(bf16[32,32,2048]{2,0,1:T(8,128)(2,1)} %all-to-all-done.2) | data formatting | bytes 8388608 | tf_op jit(solution)/shard_map/all_to_all | solution.py:16
  139.5 1.3 convolution_minimum_fusion
  140.8 2.0 fusion.22
  142.8 0.7 constant_dynamic-slice_fusion.2
  143.4 0.5 convolution_convert_fusion.3
  144.0 0.4 fusion.50
  144.3 2.3 fusion.39
  146.7 0.3 fusion.34
  147.0 0.1 convolution_bitcast_fusion.1
  147.2 13.5 %all-gather.5.cloned.1.call-done = bf16[32,256,128]{1,0,2:T(8,128)(2,1)} async-done(((bf16[16,256,128]{1,0,2:T(8,128)(2,1)}), bf16[32,256,128]{1,0,2:T(8,128)(2,1)}) %all-gather.5.cloned.1.call-update) | async-done | bytes 2097168 | tf_op jit(solution)/shard_map/all_gather | solution.py:30
  160.6 3.6 %copy.49 = bf16[2,16,256,128]{3,2,0,1:T(8,128)(2,1)S(1)} copy(bf16[2,16,256,128]{2,1,0,3:T(8,128)(2,1)} %bitcast.140) | data formatting | bytes 4194304 | tf_op jit(solution)/shard_map/reshape | solution.py:32
  164.2 4.1 %while.12 = (s32[]{:T(128)}, f32[256,1,64]{0,2,1:T(8,128)S(1)}, f32[1,256]{1,0:T(1,128)S(1)}, s32[]{:T(128)}, s32[]{:T(128)}, /*index=5*/bf16[8192,128]{1,0:T(8,...) while((s32[]{:T(128)}, f32[256,1,64]{0,2,1:T(8,128)S(1)}, ...), condition=%wide.region_8.9_spmd, body=%wide.region_4.8_spmd.sunk | while | flops 27083784 | bytes 2680031 | solution.py:118
  164.2 0.7 constant_dynamic-slice_fusion.4
  164.9 0.3 fusion.77
  165.2 2.3 fusion.78
  167.6 0.4 fusion.79
  168.0 0.3 fusion.80
  168.3 0.8 broadcast_in_dim.17
  169.2 5.5 %all-to-all-start = ((bf16[16,256,64]{1,2,0:T(8,128)(2,1)}), bf16[16,256,64]{1,2,0:T(8,128)(2,1)S(1)}, u32[]{:S(2)}, u32[]{:S(2)}) async-start(bf16[16,256,64]{1,2,0:T(8,128)(2,1)} %broadcast_in_dim.17), calls=%async_computation | async-start | bytes 1048576 | tf_op jit(solution)/shard_map/all_to_all | solution.py:43
  174.7 59.6 %all-gather.7.cloned.1.call-done = bf16[32,32,2048]{2,1,0:T(8,128)(2,1)} async-done(((bf16[32,32,128]{2,1,0:T(8,128)(2,1)}), bf16[32,32,2048]{2,1,0:T(8,128)(2,1)}) %all-gather.7.cloned.1.call-update) | async-done | bytes 4194320 | tf_op jit(solution)/shard_map/all_gather | solution.py:163
  234.3 4.3 %convolution_convert_fusion = bf16[1024,128]{1,0:T(8,128)(2,1)} fusion(bf16[1024,2048]{1,0:T(8,128)(2,1)} %bitcast.154, bf16[1,2048,128]{2,1,0:T(8,128)(2,1)} %param.29), kind=kOutput, calls=%fused_computation.40 | convolution fusion | flops 537001984 | bytes 4980736 | tf_op jit(solution)/shard_map/dot_general | solution.py:166
  238.6 73.0 %all-to-all-start.3 = ((bf16[32,32,128]{2,1,0:T(8,128)(2,1)}), bf16[32,32,128]{2,1,0:T(8,128)(2,1)S(1)}, u32[]{:S(2)}, u32[]{:S(2)}) async-start(bf16[32,32,128]{2,1,0:T(8,128)(2,1)} %bitcast.39), calls=%async_computation.3 | async-start | bytes 524288 | tf_op jit(solution)/shard_map/all_to_all | solution.py:168
  311.8 1.0 convolution_convert_fusion.1
  312.8 21.1 %all-to-all-done.3 = bf16[32,32,128]{2,1,0:T(8,128)(2,1)S(1)} async-done(((bf16[32,32,128]{2,1,0:T(8,128)(2,1)}), bf16[32,32,128]{2,1,0:T(8,128)(2,1)S(1)}, u32[]{:S(2)}, u32[]{:S(2)}) %all-to-all-start.3) | async-done | bytes 262176 | tf_op jit(solution)/shard_map/all_to_all | solution.py:168
  333.9 1.3 gather_fusion.1
  335.2 0.9 fusion.37
  (51 shorter events, 1.2 us)
Async XLA Ops:
  7.2 132.3 %copy-start = (bf16[1,2048,128]{2,1,0:T(8,128)(2,1)S(1)}, bf16[1,2048,128]{2,1,0:T(8,128)(2,1)}, u32[]{:S(2)}) copy-start(bf16[1,2048,128]{2,1,0:T(8,128)(2,1)} %param.27) | copy-start | bytes 1572868
  15.7 25.0 %copy-start.1 = (bf16[256,2048]{1,0:T(8,128)(2,1)S(1)}, bf16[256,2048]{1,0:T(8,128)(2,1)}, u32[]{:S(2)}) copy-start(bf16[256,2048]{1,0:T(8,128)(2,1)} %param.16) | copy-start | bytes 3145732
  23.9 39.0 %all-to-all-start.1 = ((bf16[32,2,2048]{2,1,0:T(2,128)(2,1)}), bf16[32,2,2048]{2,1,0:T(2,128)(2,1)S(1)}, u32[]{:S(2)}, u32[]{:S(2)}) async-start(bf16[32,2,2048]{2,1,0:T(2,128)(2,1)} %constant_dynamic-slice_fusion.1), calls=%async_computation.1 | async-start | bytes 524288 | tf_op jit(solution)/shard_map/all_to_all | solution.py:149
  65.5 7.0 %copy-start.5 = (bf16[2048,64]{0,1:T(8,128)(2,1)S(1)}, bf16[2048,64]{0,1:T(8,128)(2,1)}, u32[]{:S(2)}) copy-start(bf16[2048,64]{0,1:T(8,128)(2,1)} %param.19) | copy-start | bytes 786436
  65.5 7.0 %copy-start.8 = (f32[2048]{0:T(1024)S(1)}, f32[2048]{0:T(1024)}, u32[]{:S(2)}) copy-start(f32[2048]{0:T(1024)} %param.17) | copy-start | bytes 24580
  65.5 69.4 %all-to-all-start.2 = ((bf16[32,32,2048]{2,0,1:T(8,128)(2,1)}), bf16[32,32,2048]{2,0,1:T(8,128)(2,1)}, u32[]{:S(2)}, u32[]{:S(2)}) async-start(bf16[32,32,2048]{2,0,1:T(8,128)(2,1)} %bitcast.132), calls=%async_computation.2 | async-start | bytes 8388608 | tf_op jit(solution)/shard_map/all_to_all | solution.py:16
  72.5 1.0 copy-start.6
  72.5 58.1 %all-gather.9.cloned.1.call-start = ((), (), s32[]{:S(2)}) async-start(), calls=%async_computation.6 | async-start | bytes 1114112 | tf_op jit(solution)/shard_map/all_gather | solution.py:30
  74.6 86.0 %all-gather.5.cloned.1.call-start = ((), (), s32[]{:S(2)}) async-start(), calls=%async_computation.4 | async-start | bytes 3145728 | tf_op jit(solution)/shard_map/all_gather | solution.py:30
  133.1 101.2 %all-gather.7.cloned.1.call-start = ((), (), s32[]{:S(2)}) async-start(), calls=%async_computation.5 | async-start | bytes 4456448 | tf_op jit(solution)/shard_map/all_gather | solution.py:163
  139.5 1.3 copy-start.4
  140.7 2.7 copy-start.7
  169.2 69.5 %all-to-all-start = ((bf16[16,256,64]{1,2,0:T(8,128)(2,1)}), bf16[16,256,64]{1,2,0:T(8,128)(2,1)S(1)}, u32[]{:S(2)}, u32[]{:S(2)}) async-start(bf16[16,256,64]{1,2,0:T(8,128)(2,1)} %broadcast_in_dim.17), calls=%async_computation | async-start | bytes 1048576 | tf_op jit(solution)/shard_map/all_to_all | solution.py:43
  234.3 77.3 %copy-start.3 = (f32[128,4]{0,1:T(4,128)S(1)}, f32[128,4]{0,1:T(4,128)}, u32[]{:S(2)}) copy-start(f32[128,4]{0,1:T(4,128)} %param.26) | copy-start | bytes 6148
  234.3 77.5 %copy-start.2 = (bf16[1024,128]{1,0:T(8,128)(2,1)S(1)}, bf16[1024,128]{1,0:T(8,128)(2,1)}, u32[]{:S(2)}) copy-start(bf16[1024,128]{1,0:T(8,128)(2,1)} %param.22) | copy-start | bytes 786436
  238.6 95.3 %all-to-all-start.3 = ((bf16[32,32,128]{2,1,0:T(8,128)(2,1)}), bf16[32,32,128]{2,1,0:T(8,128)(2,1)S(1)}, u32[]{:S(2)}, u32[]{:S(2)}) async-start(bf16[32,32,128]{2,1,0:T(8,128)(2,1)} %bitcast.39), calls=%async_computation.3 | async-start | bytes 524288 | tf_op jit(solution)/shard_map/all_to_all | solution.py:168
Sparse Core Ops, SparseCore 0:
  75.9 54.6 all-gather.8
  133.2 27.3 all-gather.4
  163.6 70.6 all-gather.6
